TPU v7x, 32 devices: a whole 2x2x4 slice. The times are simulated.
32 devices in a mesh: sp: 16 (over z, y, x), tp: 2 (over core).
Axes of the slice: x: 2, y: 2, z: 4, core: 2. Of those that a mesh axis runs over, the one named last changes fastest.
Arguments:
- resid: bfloat16 [4096, 2048], P(('sp', 'tp')), may hold values from -6 to 6
- queries: bfloat16 [4096, 2048], P('sp', 'tp'), may hold values from -6 to 6
- keys: bfloat16 [4096, 1024], P('sp', 'tp'), may hold values from -6 to 6
- values: bfloat16 [4096, 1024], P('sp', 'tp'), may hold values from -6 to 6
- log_gates: float32 [16, 4096], P('tp'), as said below
- documents: int32 [4096], P('sp'), may hold values from 0 to 2, never falling along the last dimension, each value on 1 to 3072 neighbouring positions
- out_weight: bfloat16 [2048, 2048], P('tp'), may hold values from -0.125 to 0.125
- attn_gain: float32 [2048], replicated, may hold values from 0.1 to 1.9
- mlp_gain: float32 [2048], replicated, may hold values from 0.1 to 1.9
- gate_weight: bfloat16 [2048, 4096], P('sp', 'tp'), may hold values from -0.125 to 0.125
- up_weight: bfloat16 [2048, 4096], P('sp', 'tp'), may hold values from -0.125 to 0.125
- down_weight: bfloat16 [4096, 2048], P('tp', 'sp'), may hold values from -0.375 to 0.375
Outputs:
- mixed: bfloat16 [4096, 2048], P(('sp', 'tp'))
Inputs may be any that keep to these rules, and one draw needn't show every extreme that they name: `log_gates`: each head's row never rises from one position to the next and starts at or below 0. `documents`: document numbers never fall along the positions; one document spans exactly three quarters of the 4096 positions.
All inputs are finite; a program needn't handle non-finite values.
Results may differ from a plain program's by a relative error of at most 0.018.
Values may be sent and summed in bfloat16 or wider, within the bound.
A program may use at most 64 MiB of HBM per device.

v0:
```python
import math

import jax
import jax.numpy as jnp
from jax import lax
from jax.sharding import PartitionSpec as P

HD = 128


def local(
    resid,
    queries,
    keys,
    values,
    log_gates,
    documents,
    out_weight,
    attn_gain,
    mlp_gain,
    gate_weight,
    up_weight,
    down_weight,
):
    tok_rows = queries.shape[0]
    kv_dev = keys.shape[1] // HD
    heads_dev = log_gates.shape[0]
    group_size = heads_dev // kv_dev
    score_scale = 1.0 / math.sqrt(HD)
    own_start = lax.axis_index("sp") * tok_rows
    own_last = own_start + tok_rows - 1
    first_doc = documents[0]
    query_pos = own_start + lax.iota(jnp.int32, tok_rows)
    query_heads = queries.reshape(tok_rows, kv_dev, group_size, HD)
    key_gates_all = log_gates.reshape(kv_dev, group_size, log_gates.shape[1])
    query_gates = lax.dynamic_slice_in_dim(key_gates_all, own_start, tok_rows, 2)
    collected = (
        lax.all_gather(gate_weight, "sp", axis=0, tiled=True),
        lax.all_gather(up_weight, "sp", axis=0, tiled=True),
        lax.all_gather(down_weight, "sp", axis=1, tiled=True),
    )
    residual_rows = resid.astype(jnp.float32)

    def attend_block(running, key_rows, value_rows, doc_rows, first_row):
        run_max, run_sum, accumulated = running
        key_count = key_rows.shape[0]
        scores = (
            jnp.einsum(
                "tkgd,skd->kgts",
                query_heads,
                key_rows.reshape(key_count, kv_dev, HD),
                preferred_element_type=jnp.float32,
            )
            * score_scale
        )
        key_gates = lax.dynamic_slice_in_dim(key_gates_all, first_row, key_count, 2)
        scores = scores + query_gates[..., None] - key_gates[:, :, None, :]
        key_pos = first_row + lax.iota(jnp.int32, key_count)
        visible = (key_pos[None, :] <= query_pos[:, None]) & (
            doc_rows[None, :] == documents[:, None]
        )
        scores = jnp.where(visible, scores, jnp.float32(-1e30))
        new_max = jnp.maximum(run_max, jnp.max(scores, axis=-1))
        probs = jnp.where(visible, jnp.exp(scores - new_max[..., None]), jnp.float32(0.0))
        shrink = jnp.exp(run_max - new_max)
        run_sum = run_sum * shrink + jnp.sum(probs, axis=-1)
        weighted = jnp.einsum(
            "kgts,skd->kgtd",
            probs.astype(jnp.bfloat16),
            value_rows.reshape(key_count, kv_dev, HD),
            preferred_element_type=jnp.float32,
        )
        accumulated = accumulated * shrink[..., None] + weighted
        return (new_max, run_sum, accumulated)

    def maybe_attend(running, key_rows, value_rows, doc_rows, first_row):
        needed = (first_row <= own_last) & (doc_rows[-1] >= first_doc)

        def compute(state):
            return attend_block(state, key_rows, value_rows, doc_rows, first_row)

        def keep(state):
            return state

        return lax.cond(needed, compute, keep, running)

    start_state = (
        jnp.full((kv_dev, group_size, tok_rows), -1e30, jnp.float32),
        jnp.zeros((kv_dev, group_size, tok_rows), jnp.float32),
        jnp.zeros((kv_dev, group_size, tok_rows, HD), jnp.float32),
    )
    key_rows = lax.all_gather(keys, "sp", axis=0, tiled=True)
    value_rows = lax.all_gather(values, "sp", axis=0, tiled=True)
    doc_rows = lax.all_gather(documents, "sp", axis=0, tiled=True)
    key_count = key_rows.shape[0]
    block_len = math.gcd(key_count, 1024)

    def advance(block_index, inner):
        offset = block_index * block_len
        return maybe_attend(
            inner,
            lax.dynamic_slice_in_dim(key_rows, offset, block_len, 0),
            lax.dynamic_slice_in_dim(value_rows, offset, block_len, 0),
            lax.dynamic_slice_in_dim(doc_rows, offset, block_len, 0),
            offset,
        )

    run_max, run_sum, accumulated = lax.fori_loop(0, key_count // block_len, advance, start_state)
    attended = accumulated / run_sum[..., None]
    attended = (
        jnp.transpose(attended, (2, 0, 1, 3)).reshape(tok_rows, heads_dev * HD).astype(jnp.bfloat16)
    )
    rows_slice = attended
    projected = lax.psum_scatter(
        jnp.dot(rows_slice, out_weight, preferred_element_type=jnp.float32).astype(jnp.bfloat16),
        "tp",
        scatter_dimension=0,
        tiled=True,
    ).astype(jnp.float32)
    power = jnp.mean(projected * projected, axis=-1, keepdims=True)
    middle = residual_rows + attn_gain * projected * lax.rsqrt(power + 1e-06)
    middle_power = jnp.mean(middle * middle, axis=-1, keepdims=True)
    normed = (mlp_gain * middle * lax.rsqrt(middle_power + 1e-06)).astype(jnp.bfloat16)
    normed_all = lax.all_gather(normed, "tp", axis=0, tiled=True)
    gate_full, up_full, down_full = collected
    gate_act = jnp.dot(normed_all, gate_full, preferred_element_type=jnp.float32)
    up_act = jnp.dot(normed_all, up_full, preferred_element_type=jnp.float32)
    hidden = (jax.nn.silu(gate_act) * up_act).astype(jnp.bfloat16)
    rows_slice = hidden
    lowered = lax.psum_scatter(
        jnp.dot(rows_slice, down_full, preferred_element_type=jnp.float32).astype(jnp.bfloat16),
        "tp",
        scatter_dimension=0,
        tiled=True,
    ).astype(jnp.float32)
    return (middle + 0.5 * lowered).astype(jnp.bfloat16)


def solution(mesh):
    placed = (
        P(("sp", "tp"), None),
        P("sp", "tp"),
        P("sp", "tp"),
        P("sp", "tp"),
        P("tp", None),
        P("sp"),
        P("tp", None),
        P(),
        P(),
        P("sp", "tp"),
        P("sp", "tp"),
        P("tp", "sp"),
    )
    return jax.shard_map(
        local, mesh=mesh, in_specs=placed, out_specs=P(("sp", "tp"), None), check_vma=False
    )
```

profile of v0, /device:TPU:0, one launch (start us, length us, event | category | flops | bytes accessed | tf_op | source)
XLA Modules:
  0.0 660.9 jit_solution(3229841452047718858)
XLA Ops:
  6.5 1.8 copy.27
  8.3 0.0 all-gather.10.cloned.1.call-update
  8.4 0.0 all-gather.8.cloned.1.call-start
  8.4 1.8 copy.25
  10.2 0.0 all-gather.8.cloned.1.call-update
  10.2 0.0 reduce-scatter.3.cloned.1.call-start
  10.3 1.0 reshape.49
  11.3 1.2 copy.26
  12.5 0.3 copy.28
  12.8 1.2 slice.10
  14.0 43.0 %all-gather = s32[16,1,256]{2,1,0:T(1,128)S(1)} all-gather(s32[1,1,256]{2,1,0:T(1,128)} %bitcast.62), channel_id=1, replica_groups=mesh['sp'=16,'tp'=2] {'sp'}, dimensions={0}, use_global_device_ids=true | all-gather | bytes 17408 | tf_op jit(solution)/shard_map/all_gather | solution.py:94
  56.9 42.7 %all-gather.10.cloned.1.call-done = bf16[4096,512]{0,1:T(8,128)(2,1)} async-done(((bf16[256,512]{0,1:T(8,128)(2,1)}), bf16[4096,512]{0,1:T(8,128)(2,1)}) %all-gather.10.cloned.1.call-update) | async-done | bytes 4194320 | tf_op jit(solution)/shard_map/all_gather | solution.py:93
  99.7 87.7 %all-gather.8.cloned.1.call-done = bf16[4096,512]{0,1:T(8,128)(2,1)} async-done(((bf16[256,512]{0,1:T(8,128)(2,1)}), bf16[4096,512]{0,1:T(8,128)(2,1)}) %all-gather.8.cloned.1.call-update) | async-done | bytes 4194320 | tf_op jit(solution)/shard_map/all_gather | solution.py:92
  187.4 0.1 broadcast_in_dim.42
  187.5 20.5 %while.18 = (s32[]{:T(128)}, f32[4,2,256]{2,1,0:T(2,128)S(1)}, f32[4,2,256]{2,1,0:T(2,128)S(1)}, f32[4,2,256,128]{3,2,1,0:T(8,128)S(1)}, s32[]{:T(128)}, /*index...) while((s32[]{:T(128)}, f32[4,2,256]{2,1,0:T(2,128)S(1)}, ...), condition=%wide.region_5.6_spmd.clone, body=%wide.region_0.5_spmd.clone.sunk | while | flops 1114903808 | bytes 35472848 | solution.py:108
  187.5 0.6 slice.13
  189.3 13.1 %conditional.3 = ((f32[4,2,256]{2,1,0:T(2,128)S(1)}, f32[4,2,256]{2,1,0:T(2,128)S(1)}, f32[4,2,256,128]{3,2,1,0:T(8,128)S(1)})) conditional(s32[]{:T(128)} %convert_element_type.92, (f32[4,2,256]{2,1,0:T(2,128)S(1)}, f32[4,2,256]{2,1,0:T(2,128)S(1)}, f32[4,2,256,128]{3,2,1,0:T(8,128)S(1)}) %tuple.52, (s32[]{:T(128)}, s32[]{:T(128)}, ...), branch_computations={%region_1.0_spmd, %region_2.4_spmd} | conditional | flops 1114903808 | bytes 35463248 | solution.py:85
  189.4 1.0 compare_and_fusion
  190.4 1.7 constant_dynamic-slice_fusion
  192.2 3.0 fusion.6
  195.2 3.0 fusion.5
  198.3 4.1 fusion.10
  202.5 0.6 slice.13
  204.3 0.6 slice.13
  206.2 0.6 slice.13
  208.1 0.3 copy.29
  208.4 0.1 divide_convert_fusion
  208.5 4.4 convolution_convert_fusion
  213.0 0.0 all-gather.12.cloned.1.call-start
  213.0 32.7 %reduce-scatter.3.cloned.1.call-done = bf16[128,2048]{1,0:T(8,128)(2,1)} async-done(((bf16[256,2048]{1,0:T(8,128)(2,1)}), bf16[128,2048]{1,0:T(8,128)(2,1)}) %reduce-scatter.3.cloned.1.call-update) | async-done | bytes 524304 | tf_op jit(solution)/shard_map/reduce_scatter | solution.py:114
  245.7 1.2 fusion.19
  247.0 1.4 multiply_reduce_fusion
  248.4 2.2 multiply_convert_fusion
  250.6 0.0 all-gather.14.cloned.1.call-start
  250.7 0.5 all-gather.14.cloned.1.call-update
  251.2 0.0 all-gather.16.cloned.1.call-start
  251.3 0.5 all-gather.16.cloned.1.call-update
  251.8 0.0 all-gather.18.cloned.1.call-start
  251.9 0.7 all-gather.18.cloned.1.call-update
  252.6 0.2 reduce-scatter.5.cloned.1.call-start
  252.8 8.2 %all-gather.12.cloned.1.call-done = bf16[256,2048]{1,0:T(8,128)(2,1)} async-done(((bf16[128,2048]{1,0:T(8,128)(2,1)}), bf16[256,2048]{1,0:T(8,128)(2,1)}) %all-gather.12.cloned.1.call-update) | async-done | bytes 1048592 | tf_op jit(solution)/shard_map/all_gather | solution.py:124
  261.0 116.1 %all-gather.14.cloned.1.call-done = bf16[2048,2048]{1,0:T(8,128)(2,1)} async-done(((bf16[128,2048]{1,0:T(8,128)(2,1)}), bf16[2048,2048]{1,0:T(8,128)(2,1)}) %all-gather.14.cloned.1.call-update) | async-done | bytes 8388624 | tf_op jit(solution)/shard_map/all_gather | solution.py:38
  377.2 7.4 %fusion.21 = f32[256,2048]{1,0:T(8,128)} fusion(bf16[256,2048]{1,0:T(8,128)(2,1)} %all-gather.12.cloned.1.call-done, bf16[2048,2048]{1,0:T(8,128)(2,1)} %all-gather.14.cloned.1.call-done), kind=kOutput, calls=%fused_computation.39 | convolution fusion | flops 2147483648 | bytes 11534336 | tf_op jit(solution)/shard_map/dot_general | solution.py:126
  384.6 105.7 %all-gather.16.cloned.1.call-done = bf16[2048,2048]{1,0:T(8,128)(2,1)} async-done(((bf16[128,2048]{1,0:T(8,128)(2,1)}), bf16[2048,2048]{1,0:T(8,128)(2,1)}) %all-gather.16.cloned.1.call-update) | async-done | bytes 8388624 | tf_op jit(solution)/shard_map/all_gather | solution.py:39
  490.3 142.7 %all-gather.18.cloned.1.call-done = bf16[2048,2048]{1,0:T(8,128)(2,1)} async-done(((bf16[2048,128]{1,0:T(8,128)(2,1)}), bf16[2048,2048]{1,0:T(8,128)(2,1)}) %all-gather.18.cloned.1.call-update) | async-done | bytes 8388624 | tf_op jit(solution)/shard_map/all_gather | solution.py:40
  633.0 12.1 %convolution_convert_fusion.1 = bf16[256,2048]{1,0:T(8,128)(2,1)} fusion(bf16[2048,2048]{1,0:T(8,128)(2,1)} %all-gather.18.cloned.1.call-done, bf16[256,2048]{1,0:T(8,128)(2,1)S(1)} %copy-done.4, bf16[2048,2048]{1,0:T(8,128)(2,1)} %all-gather.16.cloned.1.call-done, f32[256,2048]{1,0:T(8,128)} %fusion.21), kind=kOutput, calls=%fused_computation.25 | convolution fusion | flops 4298637312 | bytes 20971520 | tf_op jit(solution)/shard_map/dot_general | solution.py:131
  645.2 6.7 %reduce-scatter.5.cloned.1.call-done = bf16[128,2048]{1,0:T(8,128)(2,1)} async-done(((bf16[256,2048]{1,0:T(8,128)(2,1)}), bf16[128,2048]{1,0:T(8,128)(2,1)}) %reduce-scatter.5.cloned.1.call-update) | async-done | bytes 524304 | tf_op jit(solution)/shard_map/reduce_scatter | solution.py:130
  651.9 2.2 add_convert_fusion
  (36 shorter events, 0.2 us)
Async XLA Ops:
  6.5 93.2 %all-gather.10.cloned.1.call-start = ((), (), s32[]{:S(2)}) async-start(), calls=%async_computation.3 | async-start | bytes 4456448 | tf_op jit(solution)/shard_map/all_gather | solution.py:93
  8.4 179.0 %all-gather.8.cloned.1.call-start = ((), (), s32[]{:S(2)}) async-start(), calls=%async_computation.2 | async-start | bytes 4456448 | tf_op jit(solution)/shard_map/all_gather | solution.py:92
  10.2 235.5 %reduce-scatter.3.cloned.1.call-start = ((), (), s32[]{:S(2)}) async-start(), calls=%async_computation.4 | async-start | bytes 1572864 | tf_op jit(solution)/shard_map/reduce_scatter | solution.py:114
  208.0 38.9 %copy-start.1 = (bf16[128,2048]{1,0:T(8,128)(2,1)S(1)}, bf16[128,2048]{1,0:T(8,128)(2,1)}, u32[]{:S(2)}) copy-start(bf16[128,2048]{1,0:T(8,128)(2,1)} %param.16) | copy-start | bytes 1572868
  208.0 38.9 %copy-start.2 = (f32[2048]{0:T(1024)S(1)}, f32[2048]{0:T(1024)}, u32[]{:S(2)}) copy-start(f32[2048]{0:T(1024)} %param.23) | copy-start | bytes 24580
  208.1 40.3 %copy-start.3 = (f32[2048]{0:T(1024)S(1)}, f32[2048]{0:T(1024)}, u32[]{:S(2)}) copy-start(f32[2048]{0:T(1024)} %param.24) | copy-start | bytes 24580
  213.0 48.1 %all-gather.12.cloned.1.call-start = ((), (), s32[]{:S(2)}) async-start(), calls=%async_computation.5 | async-start | bytes 1572864 | tf_op jit(solution)/shard_map/all_gather | solution.py:124
  250.6 126.5 %all-gather.14.cloned.1.call-start = ((), (), s32[]{:S(2)}) async-start(), calls=%async_computation.6 | async-start | bytes 8912896 | tf_op jit(solution)/shard_map/all_gather | solution.py:38
  251.2 239.1 %all-gather.16.cloned.1.call-start = ((), (), s32[]{:S(2)}) async-start(), calls=%async_computation.7 | async-start | bytes 8912896 | tf_op jit(solution)/shard_map/all_gather | solution.py:39
  251.8 381.2 %all-gather.18.cloned.1.call-start = ((), (), s32[]{:S(2)}) async-start(), calls=%async_computation.8 | async-start | bytes 8912896 | tf_op jit(solution)/shard_map/all_gather | solution.py:40
  252.6 399.4 %reduce-scatter.5.cloned.1.call-start = ((), (), s32[]{:S(2)}) async-start(), calls=%async_computation.9 | async-start | bytes 1572864 | tf_op jit(solution)/shard_map/reduce_scatter | solution.py:130
  261.0 372.0 %copy-start.4 = (bf16[256,2048]{1,0:T(8,128)(2,1)S(1)}, bf16[256,2048]{1,0:T(8,128)(2,1)}, u32[]{:S(2)}) copy-start(bf16[256,2048]{1,0:T(8,128)(2,1)} %all-gather.12.cloned.1.call-done) | copy-start | bytes 3145732
  384.6 267.3 %copy-start = (bf16[128,2048]{1,0:T(8,128)(2,1)S(1)}, bf16[128,2048]{1,0:T(8,128)(2,1)}, u32[]{:S(2)}) copy-start(bf16[128,2048]{1,0:T(8,128)(2,1)} %reduce-scatter.3.cloned.1.call-done) | copy-start | bytes 1572868
Sparse Core Ops, SparseCore 0:
  10.1 89.5 all-gather.9
  102.4 84.9 all-gather.7
  213.1 32.5 reduce-scatter.2
  250.8 10.2 all-gather.11
  263.7 113.4 all-gather.13
  379.8 110.4 all-gather.15
  493.0 139.9 all-gather.17
  645.3 6.5 reduce-scatter.4
where the time goes:
time: 662 us; the launch traced here: 661 us
  waiting for transfers between devices  545 us (82%)
  blocking collectives  43 us (6%)
  matrix products  31.2 us (5%)
  between operations  13.6 us (2%)
  local copies, waits for them, and re-layouts  11.9 us (2%)
  other arithmetic  11.2 us (2%)
    all_gather x1, waiting for transfers between devices, local(): lax.all_gather(down_weight, 'sp', axis=1, tiled=True)  143 us
    all_gather x1, waiting for transfers between devices, local(): lax.all_gather(gate_weight, 'sp', axis=0, tiled=True)  116 us
    all_gather x1, waiting for transfers between devices, local(): lax.all_gather(up_weight, 'sp', axis=0, tiled=True)  106 us
    all_gather x1, waiting for transfers between devices, local(): key_rows = lax.all_gather(keys, 'sp', axis=0, tiled=True)  87.7 us
    all_gather x1, blocking collectives, local(): doc_rows = lax.all_gather(documents, 'sp', axis=0, tiled=True)  43 us
    all_gather x1, waiting for transfers between devices, local(): value_rows = lax.all_gather(values, 'sp', axis=0, tiled=True)  42.7 us
    reduce_scatter x1, waiting for transfers between devices, local(): lax.psum_scatter(jnp.dot(rows_slice, out_weight, preferred_element_type=j...  32.7 us
  transfers between devices with their start and end apart: 8, of which 8 were waited for; matrix products, arithmetic and copies ran while one was open for 2% of the time, Pallas kernels for 0%

commit v1 on v0

--- a/solution.py
+++ b/solution.py
@@ -1,8 +1,11 @@
+import functools
 import math
 
 import jax
 import jax.numpy as jnp
 from jax import lax
+from jax.experimental import pallas as pl
+from jax.experimental.pallas import tpu as pltpu
 from jax.sharding import PartitionSpec as P
 
 HD = 128
@@ -136,6 +139,361 @@
     return (middle + 0.5 * lowered).astype(jnp.bfloat16)
 
 
+GROUP = 4
+MESH = pl.DeviceIdType.MESH
+LOG2E = 1.4426950408889634
+VMEM = pl.BlockSpec(memory_space=pltpu.VMEM)
+
+
+def greet(targets):
+    barrier = pltpu.get_barrier_semaphore()
+    for target in targets:
+        pl.semaphore_signal(barrier, inc=1, device_id=target, device_id_type=MESH)
+    pl.semaphore_wait(barrier, len(targets))
+
+
+def remote(src, dst, send_sem, recv_sem, target):
+    return pltpu.make_async_remote_copy(
+        src_ref=src,
+        dst_ref=dst,
+        send_sem=send_sem,
+        recv_sem=recv_sem,
+        device_id=target,
+        device_id_type=MESH,
+    )
+
+
+def spread_kernel(
+    plane, q_ref, k_ref, v_ref, d_ref, g_ref, u_ref, w_ref,
+    qo, ko, vo, do, go, uo, wo,
+    z_send, p_send, recv, q_send, q_recv, local_sem,
+):
+    me = lax.axis_index("sp")
+    core = lax.axis_index("tp")
+    z, p = me // plane, me % plane
+    rows = k_ref.shape[0]
+    wrows = g_ref.shape[0]
+    qcols = q_ref.shape[1] // GROUP
+    fcols = g_ref.shape[1] // GROUP
+    wcols = w_ref.shape[1]
+
+    def cols(width, index):
+        return pl.ds(pl.multiple_of(index * width, width), width)
+
+    def place(a, k):
+        if a == 0:
+            return ko.at[cols(rows, k)]
+        if a == 1:
+            return vo.at[cols(rows, k)]
+        if a == 2:
+            return do.at[k]
+        if a == 3:
+            return go.at[cols(wrows, k)]
+        if a == 4:
+            return uo.at[cols(wrows, k)]
+        return wo.at[:, cols(wcols, k)]
+
+    def piece(a, to):
+        if a == 0:
+            return k_ref.at[:, cols(HD, to)]
+        if a == 1:
+            return v_ref.at[:, cols(HD, to)]
+        if a == 2:
+            return d_ref.at[...]
+        if a == 3:
+            return g_ref.at[:, cols(fcols, to)]
+        if a == 4:
+            return u_ref.at[:, cols(fcols, to)]
+        return w_ref.at[cols(fcols, to)]
+
+    z_peers = [(z + d) % GROUP for d in range(1, GROUP)]
+    p_peers = [(p + d) % plane for d in range(1, plane)]
+    greet([(t * plane + p, core) for t in z_peers] + [(z * plane + t, core) for t in p_peers])
+    waits = []
+    keeps = []
+
+    def send_z(a):
+        for d in range(1, GROUP):
+            to = (z + d) % GROUP
+            copy = remote(piece(a, to), place(a, me), z_send.at[a, d - 1],
+                          recv.at[a, d, 0], (to * plane + p, core))
+            copy.start()
+            waits.append(copy)
+        own = pltpu.make_async_copy(piece(a, z), place(a, me), local_sem.at[a])
+        own.start()
+        keeps.append(own)
+
+    def forward(a, dz):
+        zs = (z + GROUP - dz) % GROUP
+        at = place(a, zs * plane + p)
+        if dz:
+            remote(at, at, z_send.at[a, dz - 1], recv.at[a, dz, 0], (me, core)).wait_recv()
+        else:
+            keeps[a].wait()
+        for e in range(1, plane):
+            copy = remote(at, at, p_send.at[a, dz, e - 1], recv.at[a, dz, e],
+                          (z * plane + (p + e) % plane, core))
+            copy.start()
+            waits.append(copy)
+
+    for a in (0, 1, 2):
+        send_z(a)
+    for d in range(1, GROUP):
+        to = (z + d) % GROUP
+        copy = remote(q_ref.at[:, cols(qcols, to)], qo.at[z], q_send.at[d - 1],
+                      q_recv.at[d - 1], (to * plane + p, core))
+        copy.start()
+        waits.append(copy)
+    own_q = pltpu.make_async_copy(q_ref.at[:, cols(qcols, z)], qo.at[z], local_sem.at[6])
+    own_q.start()
+    for a in (3, 4, 5):
+        send_z(a)
+    for group in ((0, 1, 2), (3, 4, 5)):
+        for dz in (0, 1, 3, 2):
+            for a in group:
+                forward(a, dz)
+    own_q.wait()
+    for copy in waits:
+        copy.wait_send()
+    for d in range(1, GROUP):
+        at = qo.at[(z + GROUP - d) % GROUP]
+        remote(at, at, q_send.at[d - 1], q_recv.at[d - 1], (me, core)).wait_recv()
+    for a in range(6):
+        for dz in range(GROUP):
+            zs = (z + GROUP - dz) % GROUP
+            for e in range(1, plane):
+                at = place(a, zs * plane + (p + plane - e) % plane)
+                remote(at, at, p_send.at[a, dz, e - 1], recv.at[a, dz, e], (me, core)).wait_recv()
+
+
+def attend_kernel(lo_ref, hi_ref, q_ref, k_ref, v_ref, gq_ref, gk_ref, dq_ref, dk_ref, pos_ref,
+                  out_ref):
+    block = 512
+    rows = q_ref.shape[1]
+    rank = q_ref.shape[2] // HD
+    coef = LOG2E / math.sqrt(HD)
+
+    def one(b, carry):
+        q = jnp.concatenate([q_ref[b, :, r * HD:(r + 1) * HD] for r in range(rank)], axis=0)
+        dq = dq_ref[b]
+        qpos = pos_ref[b]
+        gq = gq_ref[b]
+
+        def step(i, state):
+            m, l, acc = state
+            at = pl.ds(pl.multiple_of(i * block, block), block)
+            s = lax.dot_general(q, k_ref[at], (((1,), (1,)), ((), ())),
+                                preferred_element_type=jnp.float32)
+            gk = jnp.concatenate(
+                [jnp.broadcast_to(gk_ref[r:r + 1, at], (rows, block)) for r in range(rank)], axis=0)
+            s = s * coef + (gq - gk)
+            kpos = i * block + lax.broadcasted_iota(jnp.int32, (1, block), 1)
+            seen = (kpos <= qpos) & (dk_ref[0:1, at] == dq)
+            s = jnp.where(seen, s, jnp.float32(-1e30))
+            m_new = jnp.maximum(m, jnp.max(s, axis=1, keepdims=True))
+            prob = jnp.exp2(s - m_new)
+            shrink = jnp.exp2(m - m_new)
+            l = l * shrink + jnp.sum(prob, axis=1, keepdims=True)
+            acc = acc * shrink + jnp.dot(prob.astype(jnp.bfloat16), v_ref[at],
+                                         preferred_element_type=jnp.float32)
+            return m_new, l, acc
+
+        start = (jnp.full((rank * rows, 1), -1e20, jnp.float32),
+                 jnp.zeros((rank * rows, 1), jnp.float32),
+                 jnp.zeros((rank * rows, HD), jnp.float32))
+        m, l, acc = lax.fori_loop(lo_ref[b], hi_ref[b], step, start)
+        res = (acc / l).astype(jnp.bfloat16)
+        for r in range(rank):
+            out_ref[b, :, r * HD:(r + 1) * HD] = res[r * rows:(r + 1) * rows]
+        return carry
+
+    lax.fori_loop(0, q_ref.shape[0], one, 0)
+
+
+def finish_kernel(
+    plane, att_ref, ow_ref, resid_ref, ag_ref, mg_ref, gw_ref, uw_ref, dw_ref, out_ref,
+    arr, pbuf, pgot, mid, nall, hid, part, pair, red, got,
+    a_send, a_recv, t_send, t_recv, n_send, n_recv, f_send, f_recv,
+    x_send, x_recv, r_send, r_recv, local_sem,
+):
+    me = lax.axis_index("sp")
+    core = lax.axis_index("tp")
+    z, p = me // plane, me % plane
+    other = 1 - core
+    mate = (me, other)
+    width = att_ref.shape[2]
+    half = resid_ref.shape[0]
+    d_model = resid_ref.shape[1]
+    tile = 512
+
+    def there(d):
+        return (((z + d) % GROUP) * plane + p, core)
+
+    greet([there(d) for d in range(1, GROUP)] + [mate])
+    for d in range(1, GROUP):
+        remote(att_ref.at[(z + d) % GROUP], arr.at[z], a_send.at[d - 1], a_recv.at[d - 1],
+               there(d)).start()
+    own = pltpu.make_async_copy(att_ref.at[z], arr.at[z], local_sem)
+    own.start()
+    own.wait()
+    for d in range(1, GROUP):
+        at = arr.at[(z + GROUP - d) % GROUP]
+        remote(at, at, a_send.at[d - 1], a_recv.at[d - 1], mate).wait_recv()
+
+    @pl.loop(0, d_model // tile)
+    def _(j):
+        at = pl.ds(pl.multiple_of(j * tile, tile), tile)
+        total = jnp.dot(arr[0], ow_ref[0:width, at], preferred_element_type=jnp.float32)
+        for g in range(1, GROUP):
+            total += jnp.dot(arr[g], ow_ref[g * width:(g + 1) * width, at],
+                             preferred_element_type=jnp.float32)
+        pbuf[0, :, at] = total[:half].astype(jnp.bfloat16)
+        pbuf[1, :, at] = total[half:].astype(jnp.bfloat16)
+
+    swap = remote(pbuf.at[other], pgot, t_send, t_recv, mate)
+    swap.start()
+    swap.wait()
+    projected = pbuf[core].astype(jnp.float32) + pgot[...].astype(jnp.float32)
+    power = jnp.mean(projected * projected, axis=-1, keepdims=True)
+    middle = resid_ref[...].astype(jnp.float32) + ag_ref[...] * projected * lax.rsqrt(power + 1e-06)
+    mid[...] = middle
+    mpower = jnp.mean(middle * middle, axis=-1, keepdims=True)
+    nall[z, core] = (mg_ref[...] * middle * lax.rsqrt(mpower + 1e-06)).astype(jnp.bfloat16)
+    mine = nall.at[z, core]
+    for d in range(1, GROUP):
+        remote(mine, mine, n_send.at[d - 1], n_recv.at[d - 1], there(d)).start()
+    remote(mine, mine, f_send.at[0], f_recv.at[0], mate).start()
+
+    for d in (0, 1, 3, 2):
+        zb = (z + GROUP - d) % GROUP
+        here, over = nall.at[zb, core], nall.at[zb, other]
+        if d:
+            remote(here, here, n_send.at[d - 1], n_recv.at[d - 1], mate).wait_recv()
+            remote(here, here, f_send.at[d], f_recv.at[d], mate).start()
+        remote(over, over, f_send.at[d], f_recv.at[d], mate).wait_recv()
+        rows_in = jnp.concatenate([nall[zb, 0], nall[zb, 1]], axis=0)
+        ftile = 256
+        for j in range(hid.shape[1] // ftile):
+            at = slice(j * ftile, (j + 1) * ftile)
+            gate = jnp.dot(rows_in, gw_ref[:, at], preferred_element_type=jnp.float32)
+            up = jnp.dot(rows_in, uw_ref[:, at], preferred_element_type=jnp.float32)
+            hid[:, at] = (gate / (1.0 + jnp.exp(-gate)) * up).astype(jnp.bfloat16)
+
+        @pl.loop(0, d_model // tile)
+        def _(j):
+            at = pl.ds(pl.multiple_of(j * tile, tile), tile)
+            total = jnp.dot(hid[...], dw_ref[:, at], preferred_element_type=jnp.float32)
+            part[d, 0, :, at] = total[:half].astype(jnp.bfloat16)
+            part[d, 1, :, at] = total[half:].astype(jnp.bfloat16)
+
+        trade = remote(part.at[d, other], pair.at[d], x_send.at[d], x_recv.at[d], mate)
+        trade.start()
+        trade.wait()
+        both = part[d, core].astype(jnp.float32) + pair[d].astype(jnp.float32)
+        if d:
+            red[d - 1] = both.astype(jnp.bfloat16)
+            remote(red.at[d - 1], got.at[d - 1], r_send.at[d - 1], r_recv.at[d - 1],
+                   there(GROUP - d)).start()
+        else:
+            mid[...] += 0.5 * both
+
+    total = mid[...]
+    for d in range(1, GROUP):
+        at = got.at[d - 1]
+        remote(at, at, r_send.at[d - 1], r_recv.at[d - 1], mate).wait_recv()
+        total += 0.5 * got[d - 1].astype(jnp.float32)
+    out_ref[...] = total.astype(jnp.bfloat16)
+    for d in range(1, GROUP):
+        at = arr.at[0]
+        remote(att_ref.at[0], at, a_send.at[d - 1], a_recv.at[d - 1], mate).wait_send()
+        remote(mine, mine, n_send.at[d - 1], n_recv.at[d - 1], mate).wait_send()
+        remote(red.at[d - 1], got.at[d - 1], r_send.at[d - 1], r_recv.at[d - 1], mate).wait_send()
+    for d in range(GROUP):
+        here = nall.at[(z + GROUP - d) % GROUP, core]
+        remote(here, here, f_send.at[d], f_recv.at[d], mate).wait_send()
+
+
+def grouped(
+    sp, resid, queries, keys, values, log_gates, documents, out_weight, attn_gain, mlp_gain,
+    gate_weight, up_weight, down_weight,
+):
+    plane = sp // GROUP
+    rows, ff = keys.shape[0], gate_weight.shape[1] // GROUP
+    d_model = resid.shape[1]
+    tokens = rows * sp
+    qcols = queries.shape[1] // GROUP
+    rank = qcols // HD
+    bf = jnp.bfloat16
+    me = lax.axis_index("sp")
+    z, p = me // plane, me % plane
+    shape = jax.ShapeDtypeStruct
+    dma = pltpu.SemaphoreType.DMA
+    limit = 60 * 1024 * 1024
+    q4, k_all, v_all, docs, g_all, u_all, w_all = pl.pallas_call(
+        functools.partial(spread_kernel, plane),
+        out_shape=(
+            shape((GROUP, rows, qcols), bf), shape((tokens, HD), bf), shape((tokens, HD), bf),
+            shape((sp, 8, rows), jnp.int32),
+            shape((d_model, ff), bf), shape((d_model, ff), bf), shape((ff, d_model), bf),
+        ),
+        in_specs=[VMEM] * 7,
+        out_specs=[VMEM] * 7,
+        scratch_shapes=[
+            dma((6, GROUP - 1)), dma((6, GROUP, plane - 1)), dma((6, GROUP, plane)),
+            dma((GROUP - 1,)), dma((GROUP - 1,)), dma((7,)),
+        ],
+        compiler_params=pltpu.CompilerParams(
+            collective_id=0, has_side_effects=True, vmem_limit_bytes=limit),
+    )(queries, keys, values, jnp.broadcast_to(documents[None, :], (8, rows)),
+      gate_weight, up_weight, down_weight)
+
+    docs_all = docs[:, 0, :].reshape(tokens)
+    gates = lax.dynamic_slice_in_dim(log_gates, z * rank, rank, 0) * LOG2E
+    def mine(x):
+        return lax.dynamic_index_in_dim(x, p, x.ndim - 2, keepdims=False)
+    gq = mine(gates.reshape(rank, GROUP, plane, rows))
+    gq = jnp.transpose(gq, (1, 0, 2)).reshape(GROUP, rank * rows, 1)
+    dq = mine(docs_all.reshape(GROUP, plane, rows))
+    pos = mine(lax.iota(jnp.int32, tokens).reshape(GROUP, plane, rows))
+    block = 512
+    hi = (pos[:, -1] + block) // block
+    lo = jnp.sum((docs_all[None, :] < dq[:, :1]).astype(jnp.int32), axis=1) // block
+    SMEM = pl.BlockSpec(memory_space=pltpu.SMEM)
+    attended = pl.pallas_call(
+        attend_kernel,
+        out_shape=shape((GROUP, rows, qcols), bf),
+        in_specs=[SMEM, SMEM] + [VMEM] * 8,
+        out_specs=VMEM,
+        compiler_params=pltpu.CompilerParams(vmem_limit_bytes=limit),
+    )(lo, hi, q4, k_all, v_all, gq, gates, jnp.tile(dq, (1, rank))[..., None],
+      docs_all[None, :], jnp.tile(pos, (1, rank))[..., None])
+
+    half = resid.shape[0]
+    return pl.pallas_call(
+        functools.partial(finish_kernel, plane),
+        out_shape=shape(resid.shape, bf),
+        in_specs=[VMEM] * 8,
+        out_specs=VMEM,
+        scratch_shapes=[
+            pltpu.VMEM((GROUP, rows, qcols), bf),
+            pltpu.VMEM((2, half, d_model), bf),
+            pltpu.VMEM((half, d_model), bf),
+            pltpu.VMEM((half, d_model), jnp.float32),
+            pltpu.VMEM((GROUP, 2, half, d_model), bf),
+            pltpu.VMEM((rows, ff), bf),
+            pltpu.VMEM((GROUP, 2, half, d_model), bf),
+            pltpu.VMEM((GROUP, half, d_model), bf),
+            pltpu.VMEM((GROUP - 1, half, d_model), bf),
+            pltpu.VMEM((GROUP - 1, half, d_model), bf),
+            dma((GROUP - 1,)), dma((GROUP - 1,)), dma, dma,
+            dma((GROUP - 1,)), dma((GROUP - 1,)), dma((GROUP,)), dma((GROUP,)),
+            dma((GROUP,)), dma((GROUP,)), dma((GROUP - 1,)), dma((GROUP - 1,)), dma,
+        ],
+        compiler_params=pltpu.CompilerParams(
+            collective_id=1, has_side_effects=True, vmem_limit_bytes=limit),
+    )(attended, out_weight, resid, attn_gain[None, :], mlp_gain[None, :], g_all, u_all, w_all)
+
+
 def solution(mesh):
     placed = (
         P(("sp", "tp"), None),
@@ -151,6 +509,13 @@
         P("sp", "tp"),
         P("tp", "sp"),
     )
+    sp, tp = mesh.shape["sp"], mesh.shape["tp"]
+
+    def layer(*args):
+        kv_dev = args[2].shape[1] // HD
+        fits = tp == 2 and sp % GROUP == 0 and kv_dev == GROUP
+        return grouped(sp, *args) if fits else local(*args)
+
     return jax.shard_map(
-        local, mesh=mesh, in_specs=placed, out_specs=P(("sp", "tp"), None), check_vma=False
+        layer, mesh=mesh, in_specs=placed, out_specs=P(("sp", "tp"), None), check_vma=False
     )

time: 662 us -> 255 us (0.39)
  waiting for transfers between devices: 545 us -> 0 us
  Pallas kernels: 0 us -> 239 us
  blocking collectives: 43 us -> 0 us
  matrix products: 31.2 us -> 0 us
  between operations: 13.6 us -> 0.11 us
  other arithmetic: 11.2 us -> 1.73 us
    all_gather x6 -> x0, waiting for transfers between devices: 503 us -> none  [the longest x1 143 us: local(): lax.all_gather(down_weight, 'sp', axis=1, tiled=True)]
    pallas_call x0 -> x3, Pallas kernels: none -> 239 us  [the longest x1 120 us: grouped(): pl.pallas_call(functools.partial(finish_kernel, plane), out_shape=shape(r...]
    all_gather x1 -> x0, blocking collectives: 43 us -> none  [local(): doc_rows = lax.all_gather(documents, 'sp', axis=0, tiled=True)]
    reduce_scatter x2 -> x0, waiting for transfers between devices: 39.4 us -> none  [the longest x1 32.7 us: local(): lax.psum_scatter(jnp.dot(rows_slice, out_weight, preferred_element_type=j...]
    dot_general x5 -> x0, matrix products: 31.2 us -> none  [the longest x1 12.1 us: local(): jnp.dot(rows_slice, down_full, preferred_element_type=jnp.float32)]
  transfers between devices with their start and end apart: 8 -> 0, of which waited for: 8 -> 0; matrix products, arithmetic and copies ran while one was open for 2% -> 0% of each run, Pallas kernels for 0% -> 0%
where the time goes in v1:
time: 255 us; the launch traced here: 251 us
  Pallas kernels  239 us (94%)
  local copies, waits for them, and re-layouts  9.72 us (4%)
    pallas_call x1, Pallas kernels, grouped(): pl.pallas_call(functools.partial(finish_kernel, plane), out_shape=shape(r...  120 us
    pallas_call x1, Pallas kernels, grouped(): pl.pallas_call(functools.partial(spread_kernel, plane), out_shape=(shape(...  105 us
    pallas_call x1, Pallas kernels, grouped(): pl.pallas_call(attend_kernel, out_shape=shape((GROUP, rows, qcols), bf),...  14 us

profile of v1, /device:TPU:0, one launch (start us, length us, event | category | flops | bytes accessed | tf_op | source)
XLA Modules:
  0.0 250.5 jit_solution(3698492324396395290)
XLA Ops:
  0.0 1.3 broadcast_in_dim.12.d_ref
  1.3 0.9 dynamic-slice_multiply_fusion.gk_ref
  2.2 0.0 copy-start
  2.3 0.1 copy.26
  2.4 1.9 tile.21.pos_ref
  4.3 1.4 copy.27.gq_ref
  5.7 105.4 %shard_map.118 = (bf16[4,256,256]{2,1,0:T(8,128)(2,1)}, bf16[4096,128]{1,0:T(8,128)(2,1)}, bf16[4096,128]{1,0:T(8,128)(2,1)}, s32[16,8,256]{2,1,0:T(8,128)}, bf1...) custom-call(bf16[256,1024]{1,0:T(8,128)(2,1)} %q_ref.1, bf16[256,512]{1,0:T(8,128)(2,1)} %k_ref.1, ...), custom_call_target="tpu_custom_call" | custom-call | tf_op jit(solution)/shard_map/pallas_call | solution.py:432
  111.1 0.0 copy-done
  111.1 1.0 slice_reduce_fusion
  112.0 0.0 copy-start.1
  112.1 0.1 copy.23
  112.2 0.1 copy.25
  112.3 0.2 convert_reduce_fusion
  112.5 0.6 and_select_fusion
  113.1 1.9 tile.20.dq_ref
  115.0 0.0 copy-done.1
  115.0 14.0 %shard_map.119.att_ref = bf16[4,256,256]{2,1,0:T(8,128)(2,1)} custom-call(s32[4]{0:T(128)} %get-tuple-element.22.lo_ref, s32[4]{0:T(128)} %get-tuple-element.21.hi_ref, bf16[4,256,256]{2,1,0:T(8,128)(2,1)} %get-tuple-element.13.q_ref, bf16[4096,128]{1,0:T(8,128)(2,1)} %get-tuple-element.14.k_ref, bf16[4096,128]{1,0:T(8,128)(2,1)} %get-tuple-element.15.v_ref, ...), custom_call_target="tpu_custom_call" | custom-call | tf_op jit(solution)/shard_map/pallas_call | solution.py:462
  129.0 119.6 %shard_map.120 = bf16[128,2048]{1,0:T(8,128)(2,1)} custom-call(bf16[4,256,256]{2,1,0:T(8,128)(2,1)} %shard_map.119.att_ref, bf16[1024,2048]{1,0:T(8,128)(2,1)} %ow_ref.1, bf16[128,2048]{1,0:T(8,128)(2,1)} %resid_ref.1, f32[1,2048]{1,0:T(1,128)} %bitcast.23, f32[1,2048]{1,0:T(1,128)} %bitcast.24, bf16[2048,512]{1,0:T(8,128)(2,1)} %get-tuple-element.16.gw_ref, ...), custom_call_target="tpu_custom_call" | custom-call | tf_op jit(solution)/shard_map/pallas_call | solution.py:472
  248.6 1.9 copy.33
  (9 shorter events, 0.1 us)
Async XLA Ops:
  2.2 108.9 %copy-start = (f32[2,4096]{1,0:T(2,128)}, f32[2,4096]{1,0:T(2,128)S(1)}, u32[]{:S(2)}) copy-start(f32[2,4096]{1,0:T(2,128)S(1)} %dynamic-slice_multiply_fusion.gk_ref) | copy-start | bytes 98308
  112.0 3.0 %copy-start.1 = (s32[16,1,256]{2,1,0:T(1,128)}, s32[16,1,256]{2,1,0:T(1,128)S(1)}, u32[]{:S(2)}) copy-start(s32[16,1,256]{2,1,0:T(1,128)S(1)} %get-tuple-element.20) | copy-start | bytes 49156

commit v2 on v1

--- a/solution.py
+++ b/solution.py
@@ -172,10 +172,8 @@
     core = lax.axis_index("tp")
     z, p = me // plane, me % plane
     rows = k_ref.shape[0]
-    wrows = g_ref.shape[0]
     qcols = q_ref.shape[1] // GROUP
     fcols = g_ref.shape[1] // GROUP
-    wcols = w_ref.shape[1]
 
     def cols(width, index):
         return pl.ds(pl.multiple_of(index * width, width), width)
@@ -188,10 +186,8 @@
         if a == 2:
             return do.at[k]
         if a == 3:
-            return go.at[cols(wrows, k)]
-        if a == 4:
-            return uo.at[cols(wrows, k)]
-        return wo.at[:, cols(wcols, k)]
+            return go.at[cols(g_ref.shape[0], k)]
+        return (uo, wo)[a - 4].at[k // plane]
 
     def piece(a, to):
         if a == 0:
@@ -248,17 +244,22 @@
     own_q.start()
     for a in (3, 4, 5):
         send_z(a)
-    for group in ((0, 1, 2), (3, 4, 5)):
+    for group in ((0, 1, 2), (3,)):
         for dz in (0, 1, 3, 2):
             for a in group:
                 forward(a, dz)
+    for a in (4, 5):
+        keeps[a].wait()
+        for d in range(1, GROUP):
+            at = place(a, ((z + GROUP - d) % GROUP) * plane + p)
+            remote(at, at, z_send.at[a, d - 1], recv.at[a, d, 0], (me, core)).wait_recv()
     own_q.wait()
     for copy in waits:
         copy.wait_send()
     for d in range(1, GROUP):
         at = qo.at[(z + GROUP - d) % GROUP]
         remote(at, at, q_send.at[d - 1], q_recv.at[d - 1], (me, core)).wait_recv()
-    for a in range(6):
+    for a in range(4):
         for dz in range(GROUP):
             zs = (z + GROUP - dz) % GROUP
             for e in range(1, plane):
@@ -311,10 +312,10 @@
 
 
 def finish_kernel(
-    plane, att_ref, ow_ref, resid_ref, ag_ref, mg_ref, gw_ref, uw_ref, dw_ref, out_ref,
-    arr, pbuf, pgot, mid, nall, hid, part, pair, red, got,
-    a_send, a_recv, t_send, t_recv, n_send, n_recv, f_send, f_recv,
-    x_send, x_recv, r_send, r_recv, local_sem,
+    plane, att_ref, ow_ref, resid_ref, ag_ref, mg_ref, gw, uz_ref, wz_ref, out_ref,
+    uw, dw, arr, pbuf, pgot, mid, nall, hid, part, pair, red, got,
+    a_send, a_recv, t_send, t_recv, o_send, n_send, n_recv, f_send, f_recv,
+    x_send, x_recv, r_send, r_recv, w_send, w_recv, w_local, local_sem,
 ):
     me = lax.axis_index("sp")
     core = lax.axis_index("tp")
@@ -324,17 +325,34 @@
     width = att_ref.shape[2]
     half = resid_ref.shape[0]
     d_model = resid_ref.shape[1]
+    wrows, wcols = uz_ref.shape[1], wz_ref.shape[2]
     tile = 512
 
     def there(d):
         return (((z + d) % GROUP) * plane + p, core)
 
-    greet([there(d) for d in range(1, GROUP)] + [mate])
+    def near(e):
+        return (z * plane + (p + e) % plane, core)
+
+    def weight(a, k):
+        if a == 0:
+            return uw.at[pl.ds(pl.multiple_of(k * wrows, wrows), wrows)]
+        return dw.at[:, pl.ds(pl.multiple_of(k * wcols, wcols), wcols)]
+
+    greet([there(d) for d in range(1, GROUP)] + [near(e) for e in range(1, plane)] + [mate])
     for d in range(1, GROUP):
         remote(att_ref.at[(z + d) % GROUP], arr.at[z], a_send.at[d - 1], a_recv.at[d - 1],
                there(d)).start()
     own = pltpu.make_async_copy(att_ref.at[z], arr.at[z], local_sem)
     own.start()
+    staged = (uz_ref, wz_ref)
+    for a in range(2):
+        for g in range(GROUP):
+            at = weight(a, g * plane + p)
+            pltpu.make_async_copy(staged[a].at[g], at, w_local.at[a, g]).start()
+            for e in range(1, plane):
+                remote(staged[a].at[g], at, w_send.at[a, g, e - 1], w_recv.at[a, g, e - 1],
+                       near(e)).start()
     own.wait()
     for d in range(1, GROUP):
         at = arr.at[(z + GROUP - d) % GROUP]
@@ -359,58 +377,104 @@
     mid[...] = middle
     mpower = jnp.mean(middle * middle, axis=-1, keepdims=True)
     nall[z, core] = (mg_ref[...] * middle * lax.rsqrt(mpower + 1e-06)).astype(jnp.bfloat16)
-    mine = nall.at[z, core]
-    for d in range(1, GROUP):
-        remote(mine, mine, n_send.at[d - 1], n_recv.at[d - 1], there(d)).start()
-    remote(mine, mine, f_send.at[0], f_recv.at[0], mate).start()
-
-    for d in (0, 1, 3, 2):
-        zb = (z + GROUP - d) % GROUP
-        here, over = nall.at[zb, core], nall.at[zb, other]
-        if d:
-            remote(here, here, n_send.at[d - 1], n_recv.at[d - 1], mate).wait_recv()
-            remote(here, here, f_send.at[d], f_recv.at[d], mate).start()
-        remote(over, over, f_send.at[d], f_recv.at[d], mate).wait_recv()
+
+    def relay(zb, side, send_sem):
+        block = nall.at[zb, core]
+        return remote(block, block, send_sem, n_recv.at[zb],
+                      ((z + 1 - 2 * side) * plane + p, core))
+
+    def share(zb):
+        block = nall.at[zb, core]
+        return remote(block, block, f_send.at[zb], f_recv.at[zb], mate)
+
+    def onward(side):
+        return (side == 0) & (z < GROUP - 1) | (side == 1) & (z > 0)
+
+    for side in (0, 1):
+        @pl.when(onward(side))
+        def _():
+            relay(z, side, o_send.at[side]).start()
+    share(z).start()
+
+    def feed(zb):
+        over = nall.at[zb, other]
+        remote(over, over, f_send.at[zb], f_recv.at[zb], mate).wait_recv()
         rows_in = jnp.concatenate([nall[zb, 0], nall[zb, 1]], axis=0)
         ftile = 256
         for j in range(hid.shape[1] // ftile):
             at = slice(j * ftile, (j + 1) * ftile)
-            gate = jnp.dot(rows_in, gw_ref[:, at], preferred_element_type=jnp.float32)
-            up = jnp.dot(rows_in, uw_ref[:, at], preferred_element_type=jnp.float32)
+            gate = jnp.dot(rows_in, gw[:, at], preferred_element_type=jnp.float32)
+            up = jnp.dot(rows_in, uw[:, at], preferred_element_type=jnp.float32)
             hid[:, at] = (gate / (1.0 + jnp.exp(-gate)) * up).astype(jnp.bfloat16)
 
         @pl.loop(0, d_model // tile)
         def _(j):
             at = pl.ds(pl.multiple_of(j * tile, tile), tile)
-            total = jnp.dot(hid[...], dw_ref[:, at], preferred_element_type=jnp.float32)
-            part[d, 0, :, at] = total[:half].astype(jnp.bfloat16)
-            part[d, 1, :, at] = total[half:].astype(jnp.bfloat16)
-
-        trade = remote(part.at[d, other], pair.at[d], x_send.at[d], x_recv.at[d], mate)
+            total = jnp.dot(hid[...], dw[:, at], preferred_element_type=jnp.float32)
+            part[zb, 0, :, at] = total[:half].astype(jnp.bfloat16)
+            part[zb, 1, :, at] = total[half:].astype(jnp.bfloat16)
+
+        trade = remote(part.at[zb, other], pair.at[zb], x_send.at[zb], x_recv.at[zb], mate)
         trade.start()
         trade.wait()
-        both = part[d, core].astype(jnp.float32) + pair[d].astype(jnp.float32)
-        if d:
-            red[d - 1] = both.astype(jnp.bfloat16)
-            remote(red.at[d - 1], got.at[d - 1], r_send.at[d - 1], r_recv.at[d - 1],
-                   there(GROUP - d)).start()
-        else:
-            mid[...] += 0.5 * both
-
-    total = mid[...]
+        return part[zb, core].astype(jnp.float32) + pair[zb].astype(jnp.float32)
+
+    def arrive(d):
+        for side in (0, 1):
+            zb = z - d if side == 0 else z + d
+
+            @pl.when((zb >= 0) & (zb < GROUP))
+            def _():
+                block = nall.at[zb, core]
+                remote(block, block, n_send.at[zb], n_recv.at[zb], mate).wait_recv()
+                @pl.when(onward(side))
+                def _():
+                    relay(zb, side, n_send.at[zb]).start()
+                share(zb).start()
+
+    arrive(1)
+    arrive(2)
+    for a in range(2):
+        for g in range(GROUP):
+            pltpu.make_async_copy(staged[a].at[g], weight(a, g * plane + p),
+                                  w_local.at[a, g]).wait()
+            for e in range(1, plane):
+                at = weight(a, g * plane + (p + plane - e) % plane)
+                remote(staged[a].at[g], at, w_send.at[a, g, e - 1], w_recv.at[a, g, e - 1],
+                       near(e)).wait()
+    for d in (2, 1, 3):
+        if d == 3:
+            arrive(d)
+
+        @pl.loop(0, 2)
+        def _(side):
+            zb = z + (2 * side - 1) * d
+
+            @pl.when((zb >= 0) & (zb < GROUP))
+            def _():
+                red[zb] = feed(zb).astype(jnp.bfloat16)
+                remote(red.at[zb], got.at[z], r_send.at[zb], r_recv.at[z],
+                       (zb * plane + p, core)).start()
+    total = mid[...] + 0.5 * feed(z)
     for d in range(1, GROUP):
-        at = got.at[d - 1]
-        remote(at, at, r_send.at[d - 1], r_recv.at[d - 1], mate).wait_recv()
-        total += 0.5 * got[d - 1].astype(jnp.float32)
+        zb = (z + d) % GROUP
+        remote(red.at[zb], got.at[zb], r_send.at[zb], r_recv.at[zb], mate).wait()
+        total += 0.5 * got[zb].astype(jnp.float32)
     out_ref[...] = total.astype(jnp.bfloat16)
+    share(z).wait_send()
+    for side in (0, 1):
+        @pl.when(onward(side))
+        def _():
+            relay(z, side, o_send.at[side]).wait_send()
     for d in range(1, GROUP):
-        at = arr.at[0]
-        remote(att_ref.at[0], at, a_send.at[d - 1], a_recv.at[d - 1], mate).wait_send()
-        remote(mine, mine, n_send.at[d - 1], n_recv.at[d - 1], mate).wait_send()
-        remote(red.at[d - 1], got.at[d - 1], r_send.at[d - 1], r_recv.at[d - 1], mate).wait_send()
-    for d in range(GROUP):
-        here = nall.at[(z + GROUP - d) % GROUP, core]
-        remote(here, here, f_send.at[d], f_recv.at[d], mate).wait_send()
+        remote(att_ref.at[0], arr.at[0], a_send.at[d - 1], a_recv.at[d - 1], mate).wait_send()
+        share((z + d) % GROUP).wait_send()
+        for side in (0, 1):
+            zb = z - d if side == 0 else z + d
+
+            @pl.when((zb >= 0) & (zb < GROUP) & onward(side))
+            def _():
+                relay(zb, side, n_send.at[zb]).wait_send()
 
 
 def grouped(
@@ -420,6 +484,7 @@
     plane = sp // GROUP
     rows, ff = keys.shape[0], gate_weight.shape[1] // GROUP
     d_model = resid.shape[1]
+    wrows, wcols = gate_weight.shape[0], down_weight.shape[1]
     tokens = rows * sp
     qcols = queries.shape[1] // GROUP
     rank = qcols // HD
@@ -434,7 +499,8 @@
         out_shape=(
             shape((GROUP, rows, qcols), bf), shape((tokens, HD), bf), shape((tokens, HD), bf),
             shape((sp, 8, rows), jnp.int32),
-            shape((d_model, ff), bf), shape((d_model, ff), bf), shape((ff, d_model), bf),
+            shape((d_model, ff), bf), shape((GROUP, wrows, ff), bf),
+            shape((GROUP, ff, wcols), bf),
         ),
         in_specs=[VMEM] * 7,
         out_specs=[VMEM] * 7,
@@ -475,6 +541,8 @@
         in_specs=[VMEM] * 8,
         out_specs=VMEM,
         scratch_shapes=[
+            pltpu.VMEM((d_model, ff), bf),
+            pltpu.VMEM((ff, d_model), bf),
             pltpu.VMEM((GROUP, rows, qcols), bf),
             pltpu.VMEM((2, half, d_model), bf),
             pltpu.VMEM((half, d_model), bf),
@@ -483,11 +551,12 @@
             pltpu.VMEM((rows, ff), bf),
             pltpu.VMEM((GROUP, 2, half, d_model), bf),
             pltpu.VMEM((GROUP, half, d_model), bf),
-            pltpu.VMEM((GROUP - 1, half, d_model), bf),
-            pltpu.VMEM((GROUP - 1, half, d_model), bf),
+            pltpu.VMEM((GROUP, half, d_model), bf),
+            pltpu.VMEM((GROUP, half, d_model), bf),
             dma((GROUP - 1,)), dma((GROUP - 1,)), dma, dma,
-            dma((GROUP - 1,)), dma((GROUP - 1,)), dma((GROUP,)), dma((GROUP,)),
-            dma((GROUP,)), dma((GROUP,)), dma((GROUP - 1,)), dma((GROUP - 1,)), dma,
+            dma((2,)), dma((GROUP,)), dma((GROUP,)), dma((GROUP,)), dma((GROUP,)),
+            dma((GROUP,)), dma((GROUP,)), dma((GROUP,)), dma((GROUP,)),
+            dma((2, GROUP, plane - 1)), dma((2, GROUP, plane - 1)), dma((2, GROUP)), dma,
         ],
         compiler_params=pltpu.CompilerParams(
             collective_id=1, has_side_effects=True, vmem_limit_bytes=limit),

time: 255 us -> 203 us (0.80)
  the two profiles are of different devices: /device:TPU:0 before, /device:TPU:10 now
where the time goes in v2:
time: 203 us
  Pallas kernels  191 us (94%)
  local copies, waits for them, and re-layouts  9.73 us (5%)
    pallas_call x1, Pallas kernels, grouped(): pl.pallas_call(functools.partial(finish_kernel, plane), out_shape=shape(r...  109 us
    pallas_call x1, Pallas kernels, grouped(): pl.pallas_call(functools.partial(spread_kernel, plane), out_shape=(shape(...  68.8 us
    pallas_call x1, Pallas kernels, grouped(): pl.pallas_call(attend_kernel, out_shape=shape((GROUP, rows, qcols), bf),...  14 us

profile of v2, /device:TPU:10, one launch (start us, length us, event | category | flops | bytes accessed | tf_op | source)
XLA Modules:
  0.0 202.9 jit_solution(17740857426327447986)
XLA Ops:
  0.0 1.3 broadcast_in_dim.12.d_ref
  1.3 0.9 dynamic-slice_multiply_fusion.gk_ref
  2.2 0.0 copy-start
  2.3 0.1 copy.26
  2.4 1.9 tile.21.pos_ref
  4.3 1.4 copy.27.gq_ref
  5.7 68.8 %shard_map.118 = (bf16[4,256,256]{2,1,0:T(8,128)(2,1)}, bf16[4096,128]{1,0:T(8,128)(2,1)}, bf16[4096,128]{1,0:T(8,128)(2,1)}, s32[16,8,256]{2,1,0:T(8,128)}, bf1...) custom-call(bf16[256,1024]{1,0:T(8,128)(2,1)} %q_ref.1, ...), custom_call_target="tpu_custom_call" | custom-call | tf_op jit(solution)/shard_map/pallas_call | solution.py:497
  74.5 1.0 slice_reduce_fusion
  75.5 0.0 copy-start.1
  75.5 0.1 copy.23
  75.7 0.1 copy.25
  75.8 0.2 convert_reduce_fusion
  76.0 0.6 and_select_fusion
  76.6 1.9 tile.20.dq_ref
  78.5 0.0 copy-done
  78.5 0.0 copy-done.1
  78.5 14.0 %shard_map.119.att_ref = bf16[4,256,256]{2,1,0:T(8,128)(2,1)} custom-call(s32[4]{0:T(128)} %get-tuple-element.22.lo_ref, s32[4]{0:T(128)} %get-tuple-element.21.hi_ref, bf16[4,256,256]{2,1,0:T(8,128)(2,1)} %get-tuple-element.13.q_ref, bf16[4096,128]{1,0:T(8,128)(2,1)} %get-tuple-element.14.k_ref, bf16[4096,128]{1,0:T(8,128)(2,1)} %get-tuple-element.15.v_ref, ...), custom_call_target="tpu_custom_call" | custom-call | tf_op jit(solution)/shard_map/pallas_call | solution.py:528
  92.5 108.6 %shard_map.120 = bf16[128,2048]{1,0:T(8,128)(2,1)} custom-call(bf16[4,256,256]{2,1,0:T(8,128)(2,1)} %shard_map.119.att_ref, bf16[1024,2048]{1,0:T(8,128)(2,1)} %ow_ref.1, bf16[128,2048]{1,0:T(8,128)(2,1)} %resid_ref.1, f32[1,2048]{1,0:T(1,128)} %bitcast.23, f32[1,2048]{1,0:T(1,128)} %bitcast.24, bf16[2048,512]{1,0:T(8,128)(2,1)} %get-tuple-element.16.gw, ...), custom_call_target="tpu_custom_call" | custom-call | tf_op jit(solution)/shard_map/pallas_call | solution.py:538
  201.1 1.9 copy.33
  (9 shorter events, 0.1 us)
Async XLA Ops:
  2.2 76.3 %copy-start = (f32[2,4096]{1,0:T(2,128)}, f32[2,4096]{1,0:T(2,128)S(1)}, u32[]{:S(2)}) copy-start(f32[2,4096]{1,0:T(2,128)S(1)} %dynamic-slice_multiply_fusion.gk_ref) | copy-start | bytes 98308
  75.5 3.0 %copy-start.1 = (s32[16,1,256]{2,1,0:T(1,128)}, s32[16,1,256]{2,1,0:T(1,128)S(1)}, u32[]{:S(2)}) copy-start(s32[16,1,256]{2,1,0:T(1,128)S(1)} %get-tuple-element.20) | copy-start | bytes 49156
